TPU v7x, 256 devices: a whole 4x4x8 slice. The times are simulated.
256 devices in a mesh: fs: 16 (over y, x), tp: 16 (over z, core).
Axes of the slice: x: 4, y: 4, z: 8, core: 2. Of those that a mesh axis runs over, the one named last changes fastest.
Arguments:
- normed_inputs: bfloat16 [16384, 4096], P('fs', 'tp'), may hold values from -6 to 6
- query_upstream: bfloat16 [16384, 4096], P('fs', 'tp'), may hold values from -0.0625 to 0.0625
- key_upstream: bfloat16 [16384, 1024], P('fs', 'tp'), may hold values from -0.046875 to 0.046875
- head_outputs: bfloat16 [16384, 4096], P('fs', 'tp'), may hold values from -6 to 6
- branch_upstream: bfloat16 [16384, 4096], P('fs', 'tp'), may hold values from -0.0625 to 0.0625
- query_master: float32 [4096, 4096], P('fs', 'tp'), may hold values from -0.09375 to 0.09375
- key_master: float32 [4096, 1024], P('fs', 'tp'), may hold values from -0.09375 to 0.09375
- branch_master: float32 [4096, 4096], P('fs', 'tp'), may hold values from -0.09375 to 0.09375
- query_basis: bfloat16 [4096, 128], replicated, may hold values from -0.09375 to 0.09375
- key_basis: bfloat16 [4096, 128], replicated, may hold values from -0.09375 to 0.09375
- branch_basis: bfloat16 [4096, 128], replicated, may hold values from -0.09375 to 0.09375
- query_first: float32 [128, 4096], P(None, 'tp'), may hold values from -0.75 to 0.75
- query_second: float32 [128, 4096], P(None, 'tp'), may hold values from 0.001 to 0.02
- key_first: float32 [128, 1024], P(None, 'tp'), may hold values from -0.75 to 0.75
- key_second: float32 [128, 1024], P(None, 'tp'), may hold values from 0.001 to 0.02
- branch_first: float32 [4096, 128], P('fs'), may hold values from -0.75 to 0.75
- branch_second: float32 [4096, 128], P('fs'), may hold values from 0.001 to 0.02
Outputs:
- query_step: float32 [4096, 4096], P('fs', 'tp')
- key_step: float32 [4096, 1024], P('fs', 'tp')
- branch_step: float32 [4096, 4096], P('fs', 'tp')
- query_updated: float32 [4096, 4096], P('fs', 'tp')
- key_updated: float32 [4096, 1024], P('fs', 'tp')
- branch_updated: float32 [4096, 4096], P('fs', 'tp')
- query_copy: bfloat16 [4096, 4096], P(None, 'tp')
- key_copy: bfloat16 [4096, 1024], P(None, 'tp')
- branch_copy: bfloat16 [4096, 4096], P(None, 'tp')
- query_first_new: float32 [128, 4096], P(None, 'tp')
- query_second_new: float32 [128, 4096], P(None, 'tp')
- key_first_new: float32 [128, 1024], P(None, 'tp')
- key_second_new: float32 [128, 1024], P(None, 'tp')
- branch_first_new: float32 [4096, 128], P('fs')
- branch_second_new: float32 [4096, 128], P('fs')
All inputs are finite; a program needn't handle non-finite values.
Results may differ from a plain program's by a relative error of at most 0.001.
Values may be sent and summed in bfloat16 or wider, within the bound.
A program may use at most 128 MiB of HBM per device.

v0:
```python
import functools
import jax
import jax.numpy as jnp
from jax import lax
from jax.sharding import Mesh
from jax.sharding import PartitionSpec as P

FS = ("fs_0", "fs_1")
TP = ("tp_0", "tp_1")
FS_TP = ("fs_0", "fs_1", "tp_0", "tp_1")
LEARN = 0.02
BETA_ONE = 0.9
BETA_TWO = 0.95
ADAM_EPS = 1e-08
CLIP_RMS = 0.5


def together(arrays, axis):
    vector, at, outs = (jnp.concatenate([a.reshape(-1) for a in arrays]), 0, [])
    subtotal = lax.psum(vector, axis)
    for a in arrays:
        outs.append(subtotal[at : at + a.size].reshape(a.shape))
        at += a.size
    return tuple(outs)


def in_blocks(array, dim, length):
    shape = array.shape
    pieces = array.reshape(*shape[:dim], length, shape[dim] // length, *shape[dim + 1 :])
    return jnp.moveaxis(pieces, dim, 0)


def sum_at_owner(array, axis, dim):
    pieces = in_blocks(array, dim, lax.axis_size(axis))
    arrived = lax.all_to_all(pieces, axis, split_axis=0, concat_axis=0, tiled=True)
    return arrived.sum(axis=0)


def copy_for_each(array, axis):
    length = lax.axis_size(axis)
    return lax.all_to_all(
        jnp.broadcast_to(array[None], (length, *array.shape)), axis, 0, 0, tiled=True
    )


def of_everyone(array, axis):
    return copy_for_each(array, axis).sum(axis=0)


def packed_total(arrays, axis):
    ends = [0]
    for a in arrays:
        ends.append(ends[-1] + a.size)
    subtotal = of_everyone(jnp.concatenate([a.ravel() for a in arrays]), axis)
    return tuple((subtotal[b:e].reshape(a.shape) for a, b, e in zip(arrays, ends, ends[1:])))


def gathered_total(array, axis):
    pieces = lax.all_gather(array, axis)
    return pieces.sum(axis=0)


def over_axes(array, axes):
    return functools.reduce(lax.psum, axes, array)


def in_one_piece(arrays, axis, dim, along):
    ends, at = ([], 0)
    for a in arrays[:-1]:
        at += a.shape[along]
        ends.append(at)
    both = jnp.concatenate(arrays, axis=along)
    return tuple(jnp.split(lax.all_gather(both, axis, axis=dim, tiled=True), ends, axis=along))


def moments(first, second, low, clip):
    scaled = clip * low
    first_new = BETA_ONE * first + (1.0 - BETA_ONE) * scaled
    second_new = BETA_TWO * second + (1.0 - BETA_TWO) * scaled * scaled
    return (first_new, second_new, first_new / (jnp.sqrt(second_new) + ADAM_EPS))


def over_tokens(left, right, precision=None):
    return lax.dot_general(
        left,
        right,
        (((0,), (0,)), ((), ())),
        precision=precision,
        preferred_element_type=jnp.float32,
    )


def per_device(
    normed_inputs,
    query_upstream,
    key_upstream,
    head_outputs,
    branch_upstream,
    query_master,
    key_master,
    branch_master,
    query_basis,
    key_basis,
    branch_basis,
    query_first,
    query_second,
    key_first,
    key_second,
    branch_first,
    branch_second,
):
    exact = lax.Precision.HIGHEST
    row_index = lax.axis_index(FS)
    col_index = lax.axis_index(TP)
    n_rows = lax.axis_size(FS)
    n_cols = lax.axis_size(TP)
    features = normed_inputs.shape[1]
    query_local = query_upstream.shape[1]
    key_local = key_upstream.shape[1]
    rows_in = query_master.shape[0]
    rank = query_basis.shape[1]
    whole_values = lax.all_gather(head_outputs, TP, axis=1, tiled=True)
    block_query = lax.dynamic_slice_in_dim(query_basis, col_index * features, features, 0)
    block_key = lax.dynamic_slice_in_dim(key_basis, col_index * features, features, 0)
    proj_query, proj_key = together(
        (
            jnp.dot(normed_inputs, block_query, preferred_element_type=jnp.float32),
            jnp.dot(normed_inputs, block_key, preferred_element_type=jnp.float32),
        ),
        TP,
    )
    part_query = over_tokens(proj_query, query_upstream.astype(jnp.float32), exact)
    part_key = over_tokens(proj_key, key_upstream.astype(jnp.float32), exact)
    grad_branch = sum_at_owner(over_tokens(whole_values, branch_upstream), FS, 0)
    own_branch = lax.dynamic_slice_in_dim(branch_basis, col_index * features, features, 0).astype(
        jnp.float32
    )
    part_branch = jnp.dot(grad_branch, own_branch, precision=exact)
    query_low, key_low = packed_total((part_query, part_key), FS)
    branch_low = gathered_total(part_branch, TP)
    local_squares = (jnp.sum(query_low * query_low) + jnp.sum(key_low * key_low)) / n_rows
    local_squares = local_squares + jnp.sum(branch_low * branch_low) / n_cols
    total = over_axes(local_squares, FS_TP)
    entries = rank * n_cols * (2 * query_local + key_local)
    rms_value = jnp.sqrt(total / float(entries))
    clip = 1.0 / jnp.maximum(1.0, rms_value / CLIP_RMS)
    q_first, q_second, q_dir = moments(query_first, query_second, query_low, clip)
    k_first, k_second, k_dir = moments(key_first, key_second, key_low, clip)
    b_first, b_second, b_dir = moments(branch_first, branch_second, branch_low, clip)
    step_rows_query = lax.dynamic_slice_in_dim(query_basis, row_index * rows_in, rows_in, 0).astype(
        jnp.float32
    )
    step_rows_key = lax.dynamic_slice_in_dim(key_basis, row_index * rows_in, rows_in, 0).astype(
        jnp.float32
    )
    query_step = jnp.dot(step_rows_query, q_dir, precision=exact)
    key_step = jnp.dot(step_rows_key, k_dir, precision=exact)
    branch_step = jnp.dot(b_dir, own_branch.T, precision=exact)
    query_updated = query_master - LEARN * query_step
    key_updated = key_master - LEARN * key_step
    branch_updated = branch_master - LEARN * branch_step
    query_copy, key_copy, branch_copy = in_one_piece(
        (
            query_updated.astype(jnp.bfloat16),
            key_updated.astype(jnp.bfloat16),
            branch_updated.astype(jnp.bfloat16),
        ),
        FS,
        0,
        1,
    )
    return (
        query_step,
        key_step,
        branch_step,
        query_updated,
        key_updated,
        branch_updated,
        query_copy,
        key_copy,
        branch_copy,
        q_first,
        q_second,
        k_first,
        k_second,
        b_first,
        b_second,
    )


def solution(mesh):
    finer = Mesh(mesh.devices.reshape(4, 4, 8, 2), ("fs_0", "fs_1", "tp_0", "tp_1"))
    return jax.shard_map(
        per_device,
        mesh=finer,
        in_specs=(
            P(FS, TP),
            P(FS, TP),
            P(FS, TP),
            P(FS, TP),
            P(FS, TP),
            P(FS, TP),
            P(FS, TP),
            P(FS, TP),
            P(),
            P(),
            P(),
            P(None, TP),
            P(None, TP),
            P(None, TP),
            P(None, TP),
            P(FS, None),
            P(FS, None),
        ),
        out_specs=(
            P(FS, TP),
            P(FS, TP),
            P(FS, TP),
            P(FS, TP),
            P(FS, TP),
            P(FS, TP),
            P(None, TP),
            P(None, TP),
            P(None, TP),
            P(None, TP),
            P(None, TP),
            P(None, TP),
            P(None, TP),
            P(FS, None),
            P(FS, None),
        ),
        check_vma=False,
    )
```

profile of v0, /device:TPU:2, one launch (start us, length us, event | category | flops | bytes accessed | tf_op | source)
XLA Modules:
  0.0 396.6 jit_solution(3107865244808029063)
XLA Ops:
  9.3 67.5 %all-gather.5.cloned.1.call-done = bf16[1024,4096]{1,0:T(8,128)(2,1)} async-done(((bf16[1024,256]{1,0:T(8,128)(2,1)}), bf16[1024,4096]{1,0:T(8,128)(2,1)}) %all-gather.5.cloned.1.call-update) | async-done | bytes 8388624 | tf_op jit(solution)/shard_map/all_gather | solution.py:122
  76.8 7.8 %fusion.39 = f32[4096,256]{1,0:T(8,128)} fusion(bf16[1024,4096]{1,0:T(8,128)(2,1)} %all-gather.5.cloned.1.call-done, bf16[1024,256]{1,0:T(8,128)(2,1)} %param.21), kind=kOutput, calls=%fused_computation.61 | convolution fusion | flops 2147483648 | bytes 13107200 | tf_op jit(solution)/shard_map/dot_general | solution.py:84
  84.6 7.4 %all-to-all-start.1 = ((f32[16,256,256]{2,1,0:T(8,128)}), f32[16,256,256]{2,1,0:T(8,128)}, u32[]{:S(2)}, u32[]{:S(2)}) async-start(f32[16,256,256]{2,1,0:T(8,128)} %bitcast.24), calls=%async_computation.1 | async-start | bytes 8388608 | tf_op jit(solution)/shard_map/all_to_all | solution.py:35
  94.0 58.0 %all-to-all-done.1 = f32[16,256,256]{2,1,0:T(8,128)} async-done(((f32[16,256,256]{2,1,0:T(8,128)}), f32[16,256,256]{2,1,0:T(8,128)}, u32[]{:S(2)}, u32[]{:S(2)}) %all-to-all-start.1) | async-done | bytes 4194336 | tf_op jit(solution)/shard_map/all_to_all | solution.py:35
  151.9 2.5 reduce_sum.57
  154.5 1.8 fusion.23
  156.3 52.1 %all-reduce.2.cloned.1.call-done = f32[262144]{0:T(1024)} async-done(((f32[262144]{0:T(1024)}), f32[262144]{0:T(1024)}) %all-reduce.2.cloned.1.call-update) | async-done | bytes 1048592 | tf_op jit(solution)/shard_map/psum | solution.py:20
  208.4 1.6 fusion
  210.1 1.6 convolution_bitcast_fusion.2
  211.8 3.5 broadcast_in_dim.2
  215.4 7.4 %all-to-all-start = ((f32[16,1,40960]{2,1,0:T(1,128)}), f32[16,1,40960]{2,1,0:T(1,128)}, u32[]{:S(2)}, u32[]{:S(2)}) async-start(f32[16,1,40960]{2,1,0:T(1,128)} %broadcast_in_dim.2), calls=%async_computation | async-start | bytes 5242880 | tf_op jit(solution)/shard_map/all_to_all | solution.py:41
  223.0 34.4 %all-to-all-done = f32[16,1,40960]{2,1,0:T(1,128)} async-done(((f32[16,1,40960]{2,1,0:T(1,128)}), f32[16,1,40960]{2,1,0:T(1,128)}, u32[]{:S(2)}, u32[]{:S(2)}) %all-to-all-start) | async-done | bytes 2621472 | tf_op jit(solution)/shard_map/all_to_all | solution.py:41
  257.4 3.4 reduce_sum.54
  263.4 1.7 reduce_sum.58
  266.5 9.4 %psum.36 = f32[]{:T(128)} all-reduce(f32[]{:T(128)S(6)} %add.73), channel_id=1, replica_groups=mesh['fs_0'=4,'fs_1'=4,'tp_0'=8,'tp_1'=2] {'fs_0'}, use_global_device_ids=true, to_apply=%region_7.0 | all-reduce | flops 1 | bytes 8 | tf_op jit(solution)/shard_map/psum | solution.py:64
  276.0 13.9 %psum.37 = f32[]{:T(128)} all-reduce(f32[]{:T(128)} %psum.36), channel_id=1, replica_groups=mesh['fs_0'=4,'fs_1'=4,'tp_0'=8,'tp_1'=2] {'fs_1'}, use_global_device_ids=true, to_apply=%region_8.0 | all-reduce | flops 1 | bytes 8 | tf_op jit(solution)/shard_map/psum | solution.py:64
  290.1 18.4 %psum.38 = f32[]{:T(128)} all-reduce(f32[]{:T(128)} %psum.37), channel_id=1, replica_groups=mesh['fs_0'=4,'fs_1'=4,'tp_0'=8,'tp_1'=2] {'tp_0'}, use_global_device_ids=true, to_apply=%region_9.0 | all-reduce | flops 1 | bytes 8 | tf_op jit(solution)/shard_map/psum | solution.py:64
  308.5 3.3 psum.39
  312.8 1.8 fusion.36
  321.7 56.1 %all-gather.7.cloned.1.call-done = bf16[4096,576]{0,1:T(8,128)(2,1)} async-done(((bf16[256,576]{0,1:T(8,128)(2,1)}), bf16[4096,576]{0,1:T(8,128)(2,1)}) %all-gather.7.cloned.1.call-update) | async-done | bytes 4718608 | tf_op jit(solution)/shard_map/all_gather | solution.py:73
  377.8 3.9 fusion.38
  381.7 4.1 %copy.83 = bf16[4096,256]{1,0:T(8,128)(2,1)} copy(bf16[4096,256]{0,1:T(8,128)(2,1)} %get-tuple-element.81) | data formatting | bytes 4194304
  385.8 2.4 copy.82
  388.2 1.9 split.13
  (74 shorter events, 13.8 us)
Async XLA Ops:
  7.2 84.9 %copy-start = (bf16[4096,128]{1,0:T(8,128)(2,1)S(1)}, bf16[4096,128]{1,0:T(8,128)(2,1)}, u32[]{:S(2)}) copy-start(bf16[4096,128]{1,0:T(8,128)(2,1)} %param.25) | copy-start | bytes 3145732
  7.2 69.6 %all-gather.5.cloned.1.call-start = ((), (), s32[]{:S(2)}) async-start(), calls=%async_computation.3 | async-start | bytes 8912896 | tf_op jit(solution)/shard_map/all_gather | solution.py:122
  84.6 7.5 %copy-start.1 = (bf16[1024,256]{1,0:T(8,128)(2,1)S(1)}, bf16[1024,256]{1,0:T(8,128)(2,1)}, u32[]{:S(2)}) copy-start(bf16[1024,256]{1,0:T(8,128)(2,1)} %param.17) | copy-start | bytes 1572868
  84.6 67.3 %all-to-all-start.1 = ((f32[16,256,256]{2,1,0:T(8,128)}), f32[16,256,256]{2,1,0:T(8,128)}, u32[]{:S(2)}, u32[]{:S(2)}) async-start(f32[16,256,256]{2,1,0:T(8,128)} %bitcast.24), calls=%async_computation.1 | async-start | bytes 8388608 | tf_op jit(solution)/shard_map/all_to_all | solution.py:35
  92.0 116.3 %all-reduce.2.cloned.1.call-start = ((), (), s32[]{:S(2)}) async-start(), calls=%async_computation.2 | async-start | bytes 2097152 | tf_op jit(solution)/shard_map/psum | solution.py:20
  92.8 115.6 %copy-start.11 = (bf16[1024,64]{0,1:T(8,128)(2,1)S(1)}, bf16[1024,64]{0,1:T(8,128)(2,1)}, u32[]{:S(2)}) copy-start(bf16[1024,64]{0,1:T(8,128)(2,1)} %param.19) | copy-start | bytes 393220
  92.8 117.3 %copy-start.4 = (bf16[1024,256]{1,0:T(8,128)(2,1)S(1)}, bf16[1024,256]{1,0:T(8,128)(2,1)}, u32[]{:S(2)}) copy-start(bf16[1024,256]{1,0:T(8,128)(2,1)} %param.18) | copy-start | bytes 1572868
  93.9 169.5 %all-gather.9.cloned.1.call-start = ((), (), s32[]{:S(2)}) async-start(), calls=%async_computation.5 | async-start | bytes 2228224 | tf_op jit(solution)/shard_map/all_gather | solution.py:59
  211.8 11.1 %copy-start.15 = (f32[128,64]{0,1:T(8,128)S(1)}, f32[128,64]{0,1:T(8,128)}, u32[]{:S(2)}) copy-start(f32[128,64]{0,1:T(8,128)} %param.30) | copy-start | bytes 98308
  215.4 51.0 %copy-start.16 = (f32[128,64]{0,1:T(8,128)S(1)}, f32[128,64]{0,1:T(8,128)}, u32[]{:S(2)}) copy-start(f32[128,64]{0,1:T(8,128)} %param.31) | copy-start | bytes 98308
  215.4 60.5 %copy-start.7 = (f32[256,256]{1,0:T(8,128)S(1)}, f32[256,256]{1,0:T(8,128)}, u32[]{:S(2)}) copy-start(f32[256,256]{1,0:T(8,128)} %param.22) | copy-start | bytes 786436
  215.4 42.0 %all-to-all-start = ((f32[16,1,40960]{2,1,0:T(1,128)}), f32[16,1,40960]{2,1,0:T(1,128)}, u32[]{:S(2)}, u32[]{:S(2)}) async-start(f32[16,1,40960]{2,1,0:T(1,128)} %broadcast_in_dim.2), calls=%async_computation | async-start | bytes 5242880 | tf_op jit(solution)/shard_map/all_to_all | solution.py:41
  222.8 67.2 %copy-start.8 = (f32[256,256]{1,0:T(8,128)S(1)}, f32[256,256]{1,0:T(8,128)}, u32[]{:S(2)}) copy-start(f32[256,256]{1,0:T(8,128)} %param.24) | copy-start | bytes 786436
  222.8 89.8 %copy-start.12 = (f32[256,128]{1,0:T(8,128)S(1)}, f32[256,128]{1,0:T(8,128)}, u32[]{:S(2)}) copy-start(f32[256,128]{1,0:T(8,128)} %param.33) | copy-start | bytes 393220
  222.8 89.8 %copy-start.13 = (f32[256,128]{1,0:T(8,128)S(1)}, f32[256,128]{1,0:T(8,128)}, u32[]{:S(2)}) copy-start(f32[256,128]{1,0:T(8,128)} %param.32) | copy-start | bytes 393220
  222.8 89.9 %copy-start.9 = (f32[128,256]{1,0:T(8,128)S(1)}, f32[128,256]{1,0:T(8,128)}, u32[]{:S(2)}) copy-start(f32[128,256]{1,0:T(8,128)} %param.29) | copy-start | bytes 393220
  222.8 89.9 %copy-start.10 = (f32[128,256]{1,0:T(8,128)S(1)}, f32[128,256]{1,0:T(8,128)}, u32[]{:S(2)}) copy-start(f32[128,256]{1,0:T(8,128)} %param.28) | copy-start | bytes 393220
  222.8 154.9 %all-gather.7.cloned.1.call-start = ((), (), s32[]{:S(2)}) async-start(), calls=%async_computation.4 | async-start | bytes 5013504 | tf_op jit(solution)/shard_map/all_gather | solution.py:73
  223.0 89.8 %copy-start.14 = (f32[256,64]{0,1:T(8,128)S(1)}, f32[256,64]{0,1:T(8,128)}, u32[]{:S(2)}) copy-start(f32[256,64]{0,1:T(8,128)} %param.23) | copy-start | bytes 196612
  312.7 9.0 %copy-start.6 = (f32[256,128]{1,0:T(8,128)}, f32[256,128]{1,0:T(8,128)S(1)}, u32[]{:S(2)}) copy-start(f32[256,128]{1,0:T(8,128)S(1)} %get-tuple-element.84) | copy-start | bytes 393220
  312.7 69.0 %copy-start.5 = (f32[256,128]{1,0:T(8,128)}, f32[256,128]{1,0:T(8,128)S(1)}, u32[]{:S(2)}) copy-start(f32[256,128]{1,0:T(8,128)S(1)} %get-tuple-element.83) | copy-start | bytes 393220
  312.8 68.9 %copy-start.2 = (f32[128,256]{1,0:T(8,128)}, f32[128,256]{1,0:T(8,128)S(1)}, u32[]{:S(2)}) copy-start(f32[128,256]{1,0:T(8,128)S(1)} %get-tuple-element.85) | copy-start | bytes 393220
  312.8 68.9 %copy-start.3 = (f32[128,256]{1,0:T(8,128)}, f32[128,256]{1,0:T(8,128)S(1)}, u32[]{:S(2)}) copy-start(f32[128,256]{1,0:T(8,128)S(1)} %get-tuple-element.86) | copy-start | bytes 393220
Sparse Core Ops, SparseCore 0:
  9.8 66.9 all-gather.4
  95.8 112.5 all-reduce.1
  210.8 39.7 all-gather.8
  317.1 60.6 all-gather.6
where the time goes:
time: 397 us
  waiting for transfers between devices  269 us (68%)
  blocking collectives  45 us (11%)
  local copies, waits for them, and re-layouts  21.8 us (5%)
  matrix products  17.9 us (5%)
  between operations  16.8 us (4%)
  starting transfers between devices  15 us (4%)
  other arithmetic  11.4 us (3%)
    all_gather x1, waiting for transfers between devices, per_device(): whole_values = lax.all_gather(head_outputs, TP, axis=1, tiled=True)  67.5 us
    all_to_all x1, waiting for transfers between devices, sum_at_owner(): lax.all_to_all(pieces, axis, split_axis=0, concat_axis=0, tiled=True)  58 us
    all_gather x1, waiting for transfers between devices, in_one_piece(): lax.all_gather(both, axis, axis=dim, tiled=True)  56.1 us
    psum x1, waiting for transfers between devices, together(): subtotal = lax.psum(vector, axis)  52.1 us
    psum x4, blocking collectives, over_axes(): return functools.reduce(lax.psum, axes, array)  45 us
    all_to_all x1, waiting for transfers between devices, copy_for_each(): lax.all_to_all(jnp.broadcast_to(array[None], (length, *array.shape)), axi...  34.4 us
    unnamed x47, local copies, waits for them, and re-layouts  11.9 us
    dot_general x3, matrix products, over_tokens(): lax.dot_general(left, right, (((0,), (0,)), ((), ())), precision=precisio...  11.1 us
  transfers between devices with their start and end apart: 6, of which 5 were waited for; matrix products, arithmetic and copies ran while one was open for 6% of the time, Pallas kernels for 0%

commit v1 on v0

--- a/solution.py
+++ b/solution.py
@@ -17,7 +17,8 @@
 
 def together(arrays, axis):
     vector, at, outs = (jnp.concatenate([a.reshape(-1) for a in arrays]), 0, [])
-    subtotal = lax.psum(vector, axis)
+    parts = lax.all_gather(vector, axis, axis=0, tiled=False)
+    subtotal = parts.sum(axis=0)
     for a in arrays:
         outs.append(subtotal[at : at + a.size].reshape(a.shape))
         at += a.size

time: 397 us -> 386 us (0.972)
  waiting for transfers between devices: 269 us -> 183 us
  blocking collectives: 45 us -> 99.1 us
  local copies, waits for them, and re-layouts: 21.8 us -> 38.3 us
  other arithmetic: 11.4 us -> 24.5 us
  starting transfers between devices: 15 us -> 7.61 us
    all_to_all x1 -> x0, waiting for transfers between devices: 58 us -> none  [sum_at_owner(): lax.all_to_all(pieces, axis, split_axis=0, concat_axis=0, tiled=True)]
    all_to_all x0 -> x1, blocking collectives: none -> 57.1 us  [sum_at_owner(): lax.all_to_all(pieces, axis, split_axis=0, concat_axis=0, tiled=True)]
    psum x1 -> x0, waiting for transfers between devices: 52.1 us -> none  [together(): subtotal = lax.psum(vector, axis)]
    all_gather x0 -> x1, waiting for transfers between devices: none -> 29.2 us  [together(): parts = lax.all_gather(vector, axis, axis=0, tiled=False)]
    all_gather x0 -> x1, local copies, waits for them, and re-layouts: none -> 16.2 us  [together(): parts = lax.all_gather(vector, axis, axis=0, tiled=False)]
    reduce_sum x0 -> x1, other arithmetic: none -> 13.1 us  [together(): subtotal = parts.sum(axis=0)]
    all_to_all x1 -> x0, starting transfers between devices: 7.41 us -> none  [sum_at_owner(): lax.all_to_all(pieces, axis, split_axis=0, concat_axis=0, tiled=True)]
    dot_general x3, matrix products: 11.1 us -> 7.13 us  [over_tokens(): lax.dot_general(left, right, (((0,), (0,)), ((), ())), precision=precisio...]
  transfers between devices with their start and end apart: 6 -> 5, of which waited for: 5 -> 4; matrix products, arithmetic and copies ran while one was open for 6% -> 14% of each run, Pallas kernels for 0% -> 0%
where the time goes in v1:
time: 386 us; the launch traced here: 385 us
  waiting for transfers between devices  183 us (47%)
  blocking collectives  99.1 us (26%)
  local copies, waits for them, and re-layouts  38.3 us (10%)
  other arithmetic  24.5 us (6%)
  between operations  16.8 us (4%)
  matrix products  15.1 us (4%)
  starting transfers between devices  7.61 us (2%)
    all_gather x1, waiting for transfers between devices, per_device(): whole_values = lax.all_gather(head_outputs, TP, axis=1, tiled=True)  64.1 us
    all_to_all x1, blocking collectives, sum_at_owner(): lax.all_to_all(pieces, axis, split_axis=0, concat_axis=0, tiled=True)  57.1 us
    all_gather x1, waiting for transfers between devices, in_one_piece(): lax.all_gather(both, axis, axis=dim, tiled=True)  55.4 us
    psum x4, blocking collectives, over_axes(): return functools.reduce(lax.psum, axes, array)  42.1 us
    all_to_all x1, waiting for transfers between devices, copy_for_each(): lax.all_to_all(jnp.broadcast_to(array[None], (length, *array.shape)), axi...  33.8 us
    all_gather x1, waiting for transfers between devices, together(): parts = lax.all_gather(vector, axis, axis=0, tiled=False)  29.2 us
    all_gather x1, local copies, waits for them, and re-layouts, together(): parts = lax.all_gather(vector, axis, axis=0, tiled=False)  16.2 us
    reduce_sum x1, other arithmetic, together(): subtotal = parts.sum(axis=0)  13.1 us
  transfers between devices with their start and end apart: 5, of which 4 were waited for; matrix products, arithmetic and copies ran while one was open for 14% of the time, Pallas kernels for 0%

profile of v1, /device:TPU:2, one launch (start us, length us, event | category | flops | bytes accessed | tf_op | source)
XLA Modules:
  0.0 384.8 jit_solution(8350071058203103279)
XLA Ops:
  10.0 1.4 convolution_bitcast_fusion
  12.7 64.1 %all-gather.7.cloned.1.call-done = bf16[1024,4096]{1,0:T(8,128)(2,1)} async-done(((bf16[1024,256]{1,0:T(8,128)(2,1)}), bf16[1024,4096]{1,0:T(8,128)(2,1)}) %all-gather.7.cloned.1.call-update) | async-done | bytes 8388624 | tf_op jit(solution)/shard_map/all_gather | solution.py:123
  76.8 6.0 %fusion.39 = f32[4096,256]{1,0:T(8,128)S(1)} fusion(bf16[1024,4096]{1,0:T(8,128)(2,1)} %all-gather.7.cloned.1.call-done, bf16[1024,256]{1,0:T(8,128)(2,1)S(1)} %copy-done.15), kind=kOutput, calls=%fused_computation.61 | convolution fusion | flops 2147483648 | bytes 13107200 | tf_op jit(solution)/shard_map/dot_general | solution.py:85
  82.8 57.1 %all_to_all.11 = f32[16,256,256]{2,1,0:T(8,128)} all-to-all(f32[16,256,256]{2,1,0:T(8,128)S(1)} %bitcast.24), channel_id=1, replica_groups=mesh['fs_0'=4,'fs_1'=4,'tp_0'=8,'tp_1'=2] {'fs_0','fs_1'}, dimensions={0} | all-to-all | bytes 8388608 | tf_op jit(solution)/shard_map/all_to_all | solution.py:36
  139.8 2.5 reduce_sum.67
  142.3 1.8 fusion.23
  144.1 29.2 %all-gather.11.cloned.1.call-done = f32[4194304]{0:T(1024)} async-done(((f32[262144]{0:T(1024)}), f32[4194304]{0:T(1024)}) %all-gather.11.cloned.1.call-update) | async-done | bytes 16777232 | tf_op jit(solution)/shard_map/all_gather | solution.py:20
  173.3 16.2 %reshape.98 = f32[16,262144]{1,0:T(8,128)} reshape(f32[4194304]{0:T(1024)} %all-gather.11.cloned.1.call-done) | data formatting | bytes 33554432 | tf_op jit(solution)/shard_map/all_gather | solution.py:20
  189.4 13.1 %reduce_sum.63 = f32[262144]{0:T(1024)S(1)} reduce(f32[16,262144]{1,0:T(8,128)} %reshape.98, f32[]{:T(128)} %constant.11.clone.1), dimensions={0}, to_apply=%region_0.0 | reduce | flops 3932160 | bytes 17825796 | tf_op jit(solution)/shard_map/reduce_sum | solution.py:21
  203.9 3.5 broadcast_in_dim.2
  207.5 7.3 %all-to-all-start = ((f32[16,1,40960]{2,1,0:T(1,128)}), f32[16,1,40960]{2,1,0:T(1,128)}, u32[]{:S(2)}, u32[]{:S(2)}) async-start(f32[16,1,40960]{2,1,0:T(1,128)} %broadcast_in_dim.2), calls=%async_computation | async-start | bytes 5242880 | tf_op jit(solution)/shard_map/all_to_all | solution.py:42
  215.2 1.7 reduce_sum.68
  217.6 33.8 %all-to-all-done = f32[16,1,40960]{2,1,0:T(1,128)} async-done(((f32[16,1,40960]{2,1,0:T(1,128)}), f32[16,1,40960]{2,1,0:T(1,128)}, u32[]{:S(2)}, u32[]{:S(2)}) %all-to-all-start) | async-done | bytes 2621472 | tf_op jit(solution)/shard_map/all_to_all | solution.py:42
  251.4 3.4 reduce_sum.64
  258.1 9.7 %psum.28 = f32[]{:T(128)} all-reduce(f32[]{:T(128)S(6)} %add.71), channel_id=1, replica_groups=mesh['fs_0'=4,'fs_1'=4,'tp_0'=8,'tp_1'=2] {'fs_0'}, use_global_device_ids=true, to_apply=%region_7.0 | all-reduce | flops 1 | bytes 8 | tf_op jit(solution)/shard_map/psum | solution.py:65
  267.9 13.1 %psum.29 = f32[]{:T(128)} all-reduce(f32[]{:T(128)} %psum.28), channel_id=1, replica_groups=mesh['fs_0'=4,'fs_1'=4,'tp_0'=8,'tp_1'=2] {'fs_1'}, use_global_device_ids=true, to_apply=%region_8.0 | all-reduce | flops 1 | bytes 8 | tf_op jit(solution)/shard_map/psum | solution.py:65
  281.1 16.2 %psum.30 = f32[]{:T(128)} all-reduce(f32[]{:T(128)} %psum.29), channel_id=1, replica_groups=mesh['fs_0'=4,'fs_1'=4,'tp_0'=8,'tp_1'=2] {'tp_0'}, use_global_device_ids=true, to_apply=%region_9.0 | all-reduce | flops 1 | bytes 8 | tf_op jit(solution)/shard_map/psum | solution.py:65
  297.3 3.1 psum.31
  302.8 1.9 fusion.36
  310.5 55.4 %all-gather.9.cloned.1.call-done = bf16[4096,576]{0,1:T(8,128)(2,1)} async-done(((bf16[256,576]{0,1:T(8,128)(2,1)}), bf16[4096,576]{0,1:T(8,128)(2,1)}) %all-gather.9.cloned.1.call-update) | async-done | bytes 4718608 | tf_op jit(solution)/shard_map/all_gather | solution.py:74
  365.9 3.9 %fusion.38 = (bf16[4096,256]{0,1:T(8,128)(2,1)S(1)}, bf16[4096,256]{0,1:T(8,128)(2,1)}) fusion(bf16[4096,576]{0,1:T(8,128)(2,1)} %all-gather.9.cloned.1.call-done), kind=kLoop, calls=%fused_computation.60 | loop fusion | bytes 8388608 | tf_op jit(solution)/shard_map/split | solution.py:74
  369.9 4.1 %copy.97 = bf16[4096,256]{1,0:T(8,128)(2,1)} copy(bf16[4096,256]{0,1:T(8,128)(2,1)} %get-tuple-element.97) | data formatting | bytes 4194304
  373.9 2.4 copy.98
  376.4 1.9 split.13
  (73 shorter events, 15.3 us)
Async XLA Ops:
  7.2 1.2 copy-start
  7.2 69.6 %copy-start.15 = (bf16[1024,256]{1,0:T(8,128)(2,1)S(1)}, bf16[1024,256]{1,0:T(8,128)(2,1)}, u32[]{:S(2)}) copy-start(bf16[1024,256]{1,0:T(8,128)(2,1)} %param.21) | copy-start | bytes 1572868
  7.2 69.6 %all-gather.7.cloned.1.call-start = ((), (), s32[]{:S(2)}) async-start(), calls=%async_computation.2 | async-start | bytes 8912896 | tf_op jit(solution)/shard_map/all_gather | solution.py:123
  7.9 165.4 %all-gather.11.cloned.1.call-start = ((), (), s32[]{:S(2)}) async-start(), calls=%async_computation.4 | async-start | bytes 17825792 | tf_op jit(solution)/shard_map/all_gather | solution.py:20
  12.6 202.6 %all-gather.13.cloned.1.call-start = ((), (), s32[]{:S(2)}) async-start(), calls=%async_computation.5 | async-start | bytes 2228224 | tf_op jit(solution)/shard_map/all_gather | solution.py:60
  189.4 13.1 %copy-start.3 = (bf16[1024,256]{1,0:T(8,128)(2,1)S(1)}, bf16[1024,256]{1,0:T(8,128)(2,1)}, u32[]{:S(2)}) copy-start(bf16[1024,256]{1,0:T(8,128)(2,1)} %param.18) | copy-start | bytes 1572868
  189.4 13.8 %copy-start.10 = (bf16[1024,64]{0,1:T(8,128)(2,1)S(1)}, bf16[1024,64]{0,1:T(8,128)(2,1)}, u32[]{:S(2)}) copy-start(bf16[1024,64]{0,1:T(8,128)(2,1)} %param.19) | copy-start | bytes 393220
  203.9 11.1 %copy-start.6 = (f32[256,256]{1,0:T(8,128)S(1)}, f32[256,256]{1,0:T(8,128)}, u32[]{:S(2)}) copy-start(f32[256,256]{1,0:T(8,128)} %param.24) | copy-start | bytes 786436
  207.5 43.9 %all-to-all-start = ((f32[16,1,40960]{2,1,0:T(1,128)}), f32[16,1,40960]{2,1,0:T(1,128)}, u32[]{:S(2)}, u32[]{:S(2)}) async-start(f32[16,1,40960]{2,1,0:T(1,128)} %broadcast_in_dim.2), calls=%async_computation | async-start | bytes 5242880 | tf_op jit(solution)/shard_map/all_to_all | solution.py:42
  214.7 43.3 %copy-start.13 = (f32[128,64]{0,1:T(8,128)S(1)}, f32[128,64]{0,1:T(8,128)}, u32[]{:S(2)}) copy-start(f32[128,64]{0,1:T(8,128)} %param.30) | copy-start | bytes 98308
  214.7 53.1 %copy-start.14 = (f32[128,64]{0,1:T(8,128)S(1)}, f32[128,64]{0,1:T(8,128)}, u32[]{:S(2)}) copy-start(f32[128,64]{0,1:T(8,128)} %param.31) | copy-start | bytes 98308
  214.7 66.3 %copy-start.7 = (f32[256,256]{1,0:T(8,128)S(1)}, f32[256,256]{1,0:T(8,128)}, u32[]{:S(2)}) copy-start(f32[256,256]{1,0:T(8,128)} %param.22) | copy-start | bytes 786436
  214.8 86.5 %copy-start.11 = (f32[256,128]{1,0:T(8,128)S(1)}, f32[256,128]{1,0:T(8,128)}, u32[]{:S(2)}) copy-start(f32[256,128]{1,0:T(8,128)} %param.33) | copy-start | bytes 393220
  214.8 86.5 %copy-start.12 = (f32[256,128]{1,0:T(8,128)S(1)}, f32[256,128]{1,0:T(8,128)}, u32[]{:S(2)}) copy-start(f32[256,128]{1,0:T(8,128)} %param.32) | copy-start | bytes 393220
  214.8 151.1 %all-gather.9.cloned.1.call-start = ((), (), s32[]{:S(2)}) async-start(), calls=%async_computation.3 | async-start | bytes 5013504 | tf_op jit(solution)/shard_map/all_gather | solution.py:74
  215.2 87.5 %copy-start.8 = (f32[128,256]{1,0:T(8,128)S(1)}, f32[128,256]{1,0:T(8,128)}, u32[]{:S(2)}) copy-start(f32[128,256]{1,0:T(8,128)} %param.29) | copy-start | bytes 393220
  215.2 87.5 %copy-start.9 = (f32[128,256]{1,0:T(8,128)S(1)}, f32[128,256]{1,0:T(8,128)}, u32[]{:S(2)}) copy-start(f32[128,256]{1,0:T(8,128)} %param.28) | copy-start | bytes 393220
  301.4 3.3 copy-start.5
  301.4 68.5 %copy-start.4 = (f32[256,128]{1,0:T(8,128)}, f32[256,128]{1,0:T(8,128)S(1)}, u32[]{:S(2)}) copy-start(f32[256,128]{1,0:T(8,128)S(1)} %get-tuple-element.98) | copy-start | bytes 393220
  302.7 67.1 %copy-start.1 = (f32[128,256]{1,0:T(8,128)}, f32[128,256]{1,0:T(8,128)S(1)}, u32[]{:S(2)}) copy-start(f32[128,256]{1,0:T(8,128)S(1)} %get-tuple-element.100) | copy-start | bytes 393220
  302.8 67.1 %copy-start.2 = (f32[128,256]{1,0:T(8,128)}, f32[128,256]{1,0:T(8,128)S(1)}, u32[]{:S(2)}) copy-start(f32[128,256]{1,0:T(8,128)S(1)} %get-tuple-element.101) | copy-start | bytes 393220
Sparse Core Ops, SparseCore 0:
  9.8 66.9 all-gather.6
  79.2 94.0 all-gather.10
  175.7 37.9 all-gather.12
  305.9 60.0 all-gather.8
